TPU v7x, 32 devices: a whole 2x2x4 slice. The times are simulated.
32 devices in a mesh: ep: 4 (over y, x), tp: 8 (over z, core).
Axes of the slice: x: 2, y: 2, z: 4, core: 2. Of those that a mesh axis runs over, the one named last changes fastest.
Arguments:
- tokens: bfloat16 [768, 4096], P('ep', 'tp'), may hold values from -60 to 60
- norm_gain: float32 [4096], P('tp'), may hold values from 0.1 to 1.9
- norm_bias: float32 [4096], P('tp'), may hold values from -3 to 3
- expert_ids: int32 [768, 2], P('ep'), may hold values from 0 to 15, all different within a row; in each aligned block of 192 rows (0 to 191, 192 to 383, ...) at most 48 rows name the same one
- route_weights: float32 [768, 2], P('ep'), may hold values from 0.1 to 1
- gate_weight: bfloat16 [16, 4096, 4096], P('ep', None, 'tp'), may hold values from -0.375 to 0.375
- up_weight: bfloat16 [16, 4096, 4096], P('ep', None, 'tp'), may hold values from -0.375 to 0.375
- down_weight: bfloat16 [16, 4096, 4096], P('ep', None, 'tp'), may hold values from -0.01171875 to 0.01171875
Outputs:
- combined: bfloat16 [768, 4096], P('ep', 'tp')
Inputs may be any that keep to these rules, and one draw needn't show every extreme that they name: `expert_ids`: each row names 2 different experts. Among the 192 rows of one index of ep (aligned blocks of 192 rows), no expert is named more than 48 times, a bound that some block reaches.
All inputs are finite; a program needn't handle non-finite values.
Results may differ from a plain program's by a relative error of at most 0.0071.
Values may be sent and summed in bfloat16 or wider, within the bound.
A program may use at most 128 MiB of HBM per device.

v0:
```python
import functools
import math

import jax
import jax.numpy as jnp
from jax import lax
from jax.experimental import pallas as pl
from jax.experimental.pallas import tpu as pltpu
from jax.sharding import PartitionSpec as P

CAP = 48
SPLIT = 2
LAG = 2
MESH = pl.DeviceIdType.MESH

clamp_limit = 7.0
swish_alpha = 1.702
norm_epsilon = 1e-05


def clamped_unit(gate_pre, up_pre):
    gate_cut = jnp.minimum(gate_pre, clamp_limit)
    up_cut = jnp.clip(up_pre, -clamp_limit, clamp_limit)
    return gate_cut * jax.nn.sigmoid(swish_alpha * gate_cut) * (up_cut + 1.0)


def remote(src, dst, send_sem, recv_sem, device):
    return pltpu.make_async_remote_copy(
        src_ref=src,
        dst_ref=dst,
        send_sem=send_sem,
        recv_sem=recv_sem,
        device_id=device,
        device_id_type=MESH,
    )


def layer_kernel(
    side, n_tp, top,
    x_ref, gain_ref, bias_ref, ids_ref, rw_ref, gate_hbm, up_hbm, down_hbm,
    o_ref,
    tok, own_meta, meta, gains, biases, upper, wg, wu, wd, normed, routed, hid, res,
    part, ret_out, ret_in,
    w_sem, d_sem, own_sem, t_send, o_send, y_send, t_recv, g_send, g_recv, m_send, m_recv,
    h_send, h_recv, r_send, r_recv,
):
    rows, columns = x_ref.shape
    width = columns * n_tp
    local = wg.shape[0]
    chips, n_ep = n_tp // 2, side * side
    pieces = n_ep * local
    half = rows // SPLIT
    shift = local // 2
    e, t = lax.axis_index("ep"), lax.axis_index("tp")
    z, c = t // 2, t % 2
    ey, ex = e // side, e % side
    partner = z * 2 + 1 - c
    right, left = (e, t + 2), (e, t - 2)
    row_peers = [ey * side + (ex + i) % side for i in range(1, side)]
    column_peers = [((ey + i) % side) * side + ex for i in range(1, side)]
    far = [
        ((ey + j) % side) * side + (ex + i) % side
        for j in range(1, side)
        for i in range(1, side)
    ]

    def source(p):
        return ((ey + p // side) % side) * side + (ex + p % side) % side

    def cols(tt):
        return pl.ds(pl.multiple_of(tt * columns, columns), columns)

    def load_in(j):
        return (
            pltpu.make_async_copy(gate_hbm.at[j], wg.at[j], w_sem.at[0, j]),
            pltpu.make_async_copy(up_hbm.at[j], wu.at[j], w_sem.at[1, j]),
        )

    def piece_of(i):
        return (i + shift) % pieces

    def load_down(i):
        return pltpu.make_async_copy(
            down_hbm.at[piece_of(i) % local], wd.at[i % 2], d_sem.at[i % 2]
        )

    for i in range(local):
        for copy in load_in((i + shift) % local):
            copy.start()

    barrier = pltpu.get_barrier_semaphore()
    for i in range(1, n_tp):
        pl.semaphore_signal(barrier, inc=1, device_id=(e, (t + i) % n_tp), device_id_type=MESH)
    for i in range(1, n_ep):
        pl.semaphore_signal(barrier, inc=1, device_id=((e + i) % n_ep, t), device_id_type=MESH)

    a = lax.broadcasted_iota(jnp.int32, (rows, rows), 0)
    b = lax.broadcasted_iota(jnp.int32, (rows, rows), 1)
    upper[...] = (a < b).astype(jnp.float32).astype(jnp.bfloat16)
    for k in range(top):
        named = ids_ref[:, k : k + 1].astype(jnp.float32)
        own_meta[k : k + 1, :] = jnp.sum(jnp.where(a == b, named, 0.0), 0, keepdims=True)
        held = rw_ref[:, k : k + 1]
        own_meta[top + k : top + k + 1, :] = jnp.sum(
            jnp.where(a == b, held, 0.0), 0, keepdims=True
        )
    pl.semaphore_wait(barrier, n_tp - 1 + n_ep - 1)

    def lines(q):
        return pl.ds(q * half, half)

    def block(s, q, zz):
        return tok.at[s, lines(q), cols(zz * 2 + c)]

    def send(src, s, q, zz, sem, device):
        return remote(src, block(s, q, zz), sem, t_recv.at[s, q, zz * 2 + c], device)

    def to_partner(src, s, q, zz):
        return send(src, s, q, zz, t_send.at[s, q, zz], (e, partner))

    def along(src, q, zz, kind):
        return send(src, e, q, zz, o_send.at[q, zz, kind], (right, left)[kind])

    def arrived(s, q, zz):
        to_partner(block(s, q, zz), s, q, zz).wait_recv()

    def own_out(src, q, zz):
        return [
            send(src, e, q, zz, o_send.at[q, zz, 2 + i], (s, t))
            for i, s in enumerate(row_peers + column_peers)
        ] + [to_partner(src, e, q, zz)]

    def relayed(i, s, targets, q, zz):
        return [
            send(block(s, q, zz), s, q, zz, y_send.at[i, q, zz, n], (o, t))
            for n, o in enumerate(targets)
        ]

    def out(src, q, zz):
        for copy in own_out(src, q, zz):
            copy.start()

    own = []
    for q in range(SPLIT):
        src = x_ref.at[lines(q), :]

        @pl.when(z < chips - 1)
        def _():
            along(src, q, z, 0).start()

        @pl.when(z > 0)
        def _():
            along(src, q, z, 1).start()

        out(src, q, z)
        own.append(pltpu.make_async_copy(src, block(e, q, z), own_sem.at[q]))
        own[-1].start()

    gb_own = [
        pltpu.make_async_copy(gain_ref, gains.at[:, cols(t)], own_sem.at[SPLIT]),
        pltpu.make_async_copy(bias_ref, biases.at[:, cols(t)], own_sem.at[SPLIT + 1]),
        pltpu.make_async_copy(own_meta, meta.at[e], own_sem.at[SPLIT + 2]),
    ]
    for copy in gb_own:
        copy.start()

    def gb_copy(n, ref, dst, i, o):
        return remote(ref, dst.at[:, cols(o)], g_send.at[n, i], g_recv.at[n, o], (e, (t + i) % n_tp))

    def meta_copy(i, o):
        return remote(own_meta, meta.at[o], m_send.at[i], m_recv.at[o], ((e + i) % n_ep, t))

    for i in range(1, n_tp):
        gb_copy(0, gain_ref, gains, i, t).start()
        gb_copy(1, bias_ref, biases, i, t).start()
    for i in range(1, n_ep):
        meta_copy(i, e).start()
    load_down(0).start()
    load_down(1).start()

    def line_round(k):
        for q in range(SPLIT):

            @pl.when(z - k >= 0)
            def _():
                zz = z - k
                arrived(e, q, zz)

                @pl.when(z < chips - 1)
                def _():
                    along(block(e, q, zz), q, zz, 0).start()

                out(block(e, q, zz), q, zz)

            @pl.when(z + k < chips)
            def _():
                zz = z + k
                arrived(e, q, zz)

                @pl.when(z > 0)
                def _():
                    along(block(e, q, zz), q, zz, 1).start()

                out(block(e, q, zz), q, zz)

    def both(k, act):
        if k == 0:
            act(z)
        else:

            @pl.when(z - k >= 0)
            def _():
                act(z - k)

            @pl.when(z + k < chips)
            def _():
                act(z + k)

    def relay(zz):
        for q in range(SPLIT):
            for parity, peers, targets in (
                (0, row_peers, column_peers), (1, column_peers, row_peers)
            ):
                for i, s in enumerate(peers):
                    arrived(s, q, zz)

                    @pl.when(zz % 2 == parity)
                    def _():
                        for copy in relayed(i, s, targets, q, zz):
                            copy.start()

                    to_partner(block(s, q, zz), s, q, zz).start()

    def last(zz):
        for q in range(SPLIT):
            for s in far:
                arrived(s, q, zz)
                to_partner(block(s, q, zz), s, q, zz).start()

    early = max(0, chips - 3)
    for k in range(1, chips):
        line_round(k)
        if k >= 2 and k - 2 < early:
            both(k - 2, relay)
    for copy in own + gb_own:
        copy.wait()
    for i in range(1, n_tp):
        o = (t + i) % n_tp
        gb_copy(0, gain_ref, gains, i, o).wait_recv()
        gb_copy(1, bias_ref, biases, i, o).wait_recv()
    for i in range(1, n_ep):
        meta_copy(i, (e + i) % n_ep).wait_recv()

    def from_partner(s):
        for zz in range(chips):
            for q in range(SPLIT):
                other = tok.at[s, lines(q), cols(zz * 2 + 1 - c)]
                remote(
                    other, other, t_send.at[s, q, zz],
                    t_recv.at[s, q, zz * 2 + 1 - c], (e, partner),
                ).wait_recv()

    step_rows = 32 if rows % 32 == 0 else 16

    def normalise(s, slot):
        def body(r, carry):
            at = pl.ds(pl.multiple_of(r * step_rows, step_rows), step_rows)
            total = jnp.zeros((step_rows, 128), jnp.float32)
            squares = jnp.zeros((step_rows, 128), jnp.float32)
            for k in range(width // 128):
                v = tok[s, at, k * 128 : (k + 1) * 128].astype(jnp.float32)
                total = total + v
                squares = squares + v * v
            average = jnp.sum(total, 1, keepdims=True) / width
            spread = jnp.sum(squares, 1, keepdims=True) / width - average * average
            factor = jnp.broadcast_to(lax.rsqrt(spread + norm_epsilon), (step_rows, 128))
            average = jnp.broadcast_to(average, (step_rows, 128))
            for k in range(width // 128):
                here = slice(k * 128, (k + 1) * 128)
                v = tok[s, at, here].astype(jnp.float32)
                v = (v - average) * factor * gains[:, here] + biases[:, here]
                normed[slot, at, here] = v.astype(jnp.bfloat16)
            return carry

        lax.fori_loop(0, rows // step_rows, body, 0)

    def chosen(s, j):
        ids = [meta[s, k : k + 1, :] for k in range(top)]
        expert = (e * local + j).astype(jnp.float32)
        hits = [(row == expert).astype(jnp.float32) for row in ids]
        hit = functools.reduce(jnp.add, hits)
        wide = jnp.broadcast_to(hit, (16, rows)).astype(jnp.bfloat16)
        rank = jnp.dot(wide, upper[...], preferred_element_type=jnp.float32)[:1]
        line = lax.broadcasted_iota(jnp.int32, (CAP, rows), 0).astype(jnp.float32)
        match = jnp.where(line == rank, jnp.broadcast_to(hit, (CAP, rows)), 0.0)
        return match, hits

    def weights_of(s, j):
        match, hits = chosen(s, j)
        held = functools.reduce(
            jnp.add, [hits[k] * meta[s, top + k : top + k + 1, :] for k in range(top)]
        )
        return match * held

    def hid_block(u, zz):
        return hid.at[u, :, cols(zz * 2 + c)]

    def h_copy(u, zz, kind, device):
        return remote(
            hid_block(u, zz), hid_block(u, zz),
            h_send.at[u, zz, kind], h_recv.at[u, zz * 2 + c], device,
        )

    def compute(u):
        p, j = u // local, u % local
        s = source(p)
        slot = jnp.minimum(p, 1)
        match, _ = chosen(s, j)
        match = match.astype(jnp.bfloat16)
        wide = min(512, width)

        def pick(k, carry):
            here = pl.ds(pl.multiple_of(k * wide, wide), wide)
            routed[:, here] = jnp.dot(
                match, normed[slot, :, here], preferred_element_type=jnp.float32
            ).astype(jnp.bfloat16)
            return carry

        lax.fori_loop(0, width // wide, pick, 0)
        gate = jnp.dot(routed[...], wg[j], preferred_element_type=jnp.float32)
        up = jnp.dot(routed[...], wu[j], preferred_element_type=jnp.float32)
        hid[u, :, cols(t)] = clamped_unit(gate, up).astype(jnp.bfloat16)

        @pl.when(z < chips - 1)
        def _():
            h_copy(u, z, 1, right).start()

        @pl.when(z > 0)
        def _():
            h_copy(u, z, 2, left).start()

        h_copy(u, z, 0, (e, partner)).start()

    def hidden_round(u, k):
        @pl.when(z - k >= 0)
        def _():
            zz = z - k
            h_copy(u, zz, 0, (e, partner)).wait_recv()

            @pl.when(z < chips - 1)
            def _():
                h_copy(u, zz, 1, right).start()

            h_copy(u, zz, 0, (e, partner)).start()

        @pl.when(z + k < chips)
        def _():
            zz = z + k
            h_copy(u, zz, 0, (e, partner)).wait_recv()

            @pl.when(z > 0)
            def _():
                h_copy(u, zz, 2, left).start()

            h_copy(u, zz, 0, (e, partner)).start()

    def hidden_full(u):
        for zz in range(chips):
            other = hid.at[u, :, cols(zz * 2 + 1 - c)]
            remote(
                other, other, h_send.at[u, zz, 0], h_recv.at[u, zz * 2 + 1 - c], (e, partner)
            ).wait_recv()

    def combine(p):
        s = source(p)
        mix = [weights_of(s, j) for j in range(local)]
        mix = mix[0] if local == 1 else jnp.concatenate(mix, 0)
        high = mix.astype(jnp.bfloat16)
        low = (mix - high.astype(jnp.float32)).astype(jnp.bfloat16)
        dims = (((0,), (0,)), ((), ()))
        outs = res[p]
        part[...] = lax.dot_general(
            high, outs, dims, preferred_element_type=jnp.float32
        ) + lax.dot_general(low, outs, dims, preferred_element_type=jnp.float32)

    def ret_copy(p, s, o):
        return remote(ret_out.at[p], ret_in.at[o], r_send.at[p], r_recv.at[o], (s, t))

    def down(i):
        u = piece_of(i)
        p, j = u // local, u % local
        hidden_full(u)
        load_down(i).wait()
        made = jnp.dot(hid[u], wd[i % 2], preferred_element_type=jnp.float32)
        res[p, pl.ds(pl.multiple_of(j * CAP, CAP), CAP), :] = made.astype(jnp.bfloat16)

        @pl.when(i + 2 < pieces)
        def _():
            load_down(i + 2).start()

        @pl.when((p > 0) & (j == local - 1))
        def _():
            combine(p)
            ret_out[p] = part[...].astype(jnp.bfloat16)
            ret_copy(p, source(p), e).start()

    lead = (chips - 1) * LAG + 1
    first_other = local - shift
    first_far = (side + 1) * local - shift
    relays = [(min(k - early, first_other - 1), k) for k in range(early, chips)]
    lasts = [(max(first_far - chips + k, first_other - 1), k) for k in range(chips)]

    def step(i, carry):
        @pl.when(i < pieces)
        def _():
            u = piece_of(i)
            p, j = u // local, u % local

            @pl.when(((j == 0) & (p > 0)) | (i == 0))
            def _():
                s = source(p)
                from_partner(s)
                normalise(s, jnp.minimum(p, 1))

            @pl.when(i < local)
            def _():
                for copy in load_in(j):
                    copy.wait()

            compute(u)

        for k in range(1, chips):
            ii = i - k * LAG

            @pl.when((ii >= 0) & (ii < pieces))
            def _():
                hidden_round(piece_of(ii), k)

        for act, places in ((relay, relays), (last, lasts)):
            for at in sorted({place for place, _ in places}):

                @pl.when(i == at)
                def _():
                    for place, k in places:
                        if place == at:
                            both(k, act)

        @pl.when(i >= lead)
        def _():
            down(i - lead)

        return carry

    lax.fori_loop(0, pieces + lead, step, 0)

    combine(0)
    total = part[...]
    for i in range(1, n_ep):
        o = (e + i) % n_ep
        ret_copy(i, o, o).wait_recv()
        total = total + ret_in[o].astype(jnp.float32)
    o_ref[...] = total.astype(jnp.bfloat16)

    for p in range(1, n_ep):
        ret_copy(p, source(p), e).wait_send()
        meta_copy(p, e).wait_send()
    for i in range(1, n_tp):
        gb_copy(0, gain_ref, gains, i, t).wait_send()
        gb_copy(1, bias_ref, biases, i, t).wait_send()
    for q in range(SPLIT):
        for zz in range(chips):
            for s in range(n_ep):
                to_partner(block(s, q, zz), s, q, zz).wait_send()

            @pl.when((zz <= z) & (z < chips - 1))
            def _():
                along(block(e, q, zz), q, zz, 0).wait_send()

            @pl.when((zz >= z) & (z > 0))
            def _():
                along(block(e, q, zz), q, zz, 1).wait_send()

            for copy in own_out(block(e, q, zz), q, zz)[:-1]:
                copy.wait_send()
            peers, targets = (row_peers, column_peers)[:: 1 - 2 * (zz % 2)]
            for i, s in enumerate(peers):
                for copy in relayed(i, s, targets, q, zz):
                    copy.wait_send()

    def sent(u, carry):
        for zz in range(chips):
            h_copy(u, zz, 0, (e, partner)).wait_send()

            @pl.when((zz <= z) & (z < chips - 1))
            def _():
                h_copy(u, zz, 1, right).wait_send()

            @pl.when((zz >= z) & (z > 0))
            def _():
                h_copy(u, zz, 2, left).wait_send()

        return carry

    lax.fori_loop(0, pieces, sent, 0)


def on_device(
    n_ep, n_tp,
    tokens, norm_gain, norm_bias, expert_ids, route_weights, gate_weight, up_weight, down_weight,
):
    rows, columns = tokens.shape
    top = expert_ids.shape[1]
    local = gate_weight.shape[0]
    side = math.isqrt(n_ep)
    chips = n_tp // 2
    width = columns * n_tp
    pieces = n_ep * local
    vmem = pl.BlockSpec(memory_space=pltpu.VMEM)
    anywhere = pl.BlockSpec(memory_space=pl.ANY)
    bf16, f32, dma = jnp.bfloat16, jnp.float32, pltpu.SemaphoreType.DMA
    return pl.pallas_call(
        functools.partial(layer_kernel, side, n_tp, top),
        out_shape=jax.ShapeDtypeStruct((rows, columns), bf16),
        in_specs=[vmem] * 5 + [anywhere] * 3,
        out_specs=vmem,
        scratch_shapes=[
            pltpu.VMEM((n_ep, rows, width), bf16),
            pltpu.VMEM((8, rows), f32),
            pltpu.VMEM((n_ep, 8, rows), f32),
            pltpu.VMEM((1, width), f32),
            pltpu.VMEM((1, width), f32),
            pltpu.VMEM((rows, rows), bf16),
            pltpu.VMEM((local, width, columns), bf16),
            pltpu.VMEM((local, width, columns), bf16),
            pltpu.VMEM((2, width, columns), bf16),
            pltpu.VMEM((2, rows, width), bf16),
            pltpu.VMEM((CAP, width), bf16),
            pltpu.VMEM((pieces, CAP, width), bf16),
            pltpu.VMEM((n_ep, local * CAP, columns), bf16),
            pltpu.VMEM((rows, columns), f32),
            pltpu.VMEM((n_ep, rows, columns), bf16),
            pltpu.VMEM((n_ep, rows, columns), bf16),
            dma((2, local)),
            dma((2,)),
            dma((SPLIT + 3,)),
            dma((n_ep, SPLIT, chips)),
            dma((SPLIT, chips, 2 * side)),
            dma((side - 1, SPLIT, chips, side - 1)),
            dma((n_ep, SPLIT, n_tp)),
            dma((2, n_tp)),
            dma((2, n_tp)),
            dma((n_ep,)),
            dma((n_ep,)),
            dma((pieces, chips, 3)),
            dma((pieces, n_tp)),
            dma((n_ep,)),
            dma((n_ep,)),
        ],
        compiler_params=pltpu.CompilerParams(
            collective_id=0, has_side_effects=True, vmem_limit_bytes=66_000_000
        ),
    )(
        tokens, norm_gain.reshape(1, columns), norm_bias.reshape(1, columns),
        expert_ids, route_weights, gate_weight, up_weight, down_weight,
    )


def solution(mesh):
    n_ep, n_tp = mesh.shape["ep"], mesh.shape["tp"]
    placed = (
        P("ep", "tp"),
        P("tp"),
        P("tp"),
        P("ep", None),
        P("ep", None),
        P("ep", None, "tp"),
        P("ep", None, "tp"),
        P("ep", None, "tp"),
    )
    return jax.shard_map(
        functools.partial(on_device, n_ep, n_tp),
        mesh=mesh,
        in_specs=placed,
        out_specs=P("ep", "tp"),
        check_vma=False,
    )
```

profile of v0, /device:TPU:0, one launch (start us, length us, event | category | flops | bytes accessed | tf_op | source)
XLA Modules:
  0.0 115.3 jit_solution(3445781386957729910)
XLA Ops:
  0.0 1.4 %copy.9.ids_ref = s32[192,2]{1,0:T(8,128)} copy(s32[192,2]{0,1:T(2,128)} %param.11) | data formatting | bytes 3072 | tf_op args[3]
  1.4 1.4 %copy.10.rw_ref = f32[192,2]{1,0:T(8,128)} copy(f32[192,2]{0,1:T(2,128)} %param.12) | data formatting | bytes 3072 | tf_op args[4]
  2.9 110.8 %shard_map.82 = bf16[192,512]{1,0:T(8,128)(2,1)} custom-call(bf16[192,512]{1,0:T(8,128)(2,1)} %x_ref.1, f32[1,512]{1,0:T(1,128)} %bitcast.2, f32[1,512]{1,0:T(1,128)} %bitcast.3, s32[192,2]{1,0:T(8,128)} %copy.9.ids_ref, f32[192,2]{1,0:T(8,128)} %copy.10.rw_ref, bf16[4,4096,512]{2,1,0:T(8,128)(2,1)} %gate_hbm.1, bf16[4,4096,512]{2,1,0:T(8,128)(2,1)} %up_hbm.1, ...), custom_call_target="tpu_custom_call" | custom-call | tf_op jit(solution)/shard_map/pallas_call | solution.py:521
  113.7 1.6 %copy.12 = bf16[192,512]{1,0:T(8,128)(2,1)} copy(bf16[192,512]{1,0:T(8,128)(2,1)} %shard_map.82) | data formatting | bytes 393216
where the time goes:
time: 116 us; the launch traced here: 115 us
  Pallas kernels  111 us (96%)
  local copies, waits for them, and re-layouts  4.5 us (4%)
    pallas_call x1, Pallas kernels, on_device(): pl.pallas_call(functools.partial(layer_kernel, side, n_tp, top), out_shap...  111 us
    unnamed x3, local copies, waits for them, and re-layouts  4.5 us

commit v1 on v0

--- a/solution.py
+++ b/solution.py
@@ -11,6 +11,8 @@
 CAP = 48
 SPLIT = 2
 LAG = 2
+SHIFT = 1
+PICK = 1024
 MESH = pl.DeviceIdType.MESH
 
 clamp_limit = 7.0
@@ -50,7 +52,7 @@
     chips, n_ep = n_tp // 2, side * side
     pieces = n_ep * local
     half = rows // SPLIT
-    shift = local // 2
+    shift = min(SHIFT, local - 1)
     e, t = lax.axis_index("ep"), lax.axis_index("tp")
     z, c = t // 2, t % 2
     ey, ex = e // side, e % side
@@ -97,13 +99,8 @@
     a = lax.broadcasted_iota(jnp.int32, (rows, rows), 0)
     b = lax.broadcasted_iota(jnp.int32, (rows, rows), 1)
     upper[...] = (a < b).astype(jnp.float32).astype(jnp.bfloat16)
-    for k in range(top):
-        named = ids_ref[:, k : k + 1].astype(jnp.float32)
-        own_meta[k : k + 1, :] = jnp.sum(jnp.where(a == b, named, 0.0), 0, keepdims=True)
-        held = rw_ref[:, k : k + 1]
-        own_meta[top + k : top + k + 1, :] = jnp.sum(
-            jnp.where(a == b, held, 0.0), 0, keepdims=True
-        )
+    own_meta[:top, :] = ids_ref[...].astype(jnp.float32)
+    own_meta[top : 2 * top, :] = rw_ref[...]
     pl.semaphore_wait(barrier, n_tp - 1 + n_ep - 1)
 
     def lines(q):
@@ -262,7 +259,7 @@
 
     step_rows = 32 if rows % 32 == 0 else 16
 
-    def normalise(s, slot):
+    def normalise(s):
         def body(r, carry):
             at = pl.ds(pl.multiple_of(r * step_rows, step_rows), step_rows)
             total = jnp.zeros((step_rows, 128), jnp.float32)
@@ -279,7 +276,7 @@
                 here = slice(k * 128, (k + 1) * 128)
                 v = tok[s, at, here].astype(jnp.float32)
                 v = (v - average) * factor * gains[:, here] + biases[:, here]
-                normed[slot, at, here] = v.astype(jnp.bfloat16)
+                normed[at, here] = v.astype(jnp.bfloat16)
             return carry
 
         lax.fori_loop(0, rows // step_rows, body, 0)
@@ -302,6 +299,21 @@
         )
         return match * held
 
+    def pick(s, slot):
+        match = [chosen(s, j)[0] for j in range(local)]
+        match = match[0] if local == 1 else jnp.concatenate(match, 0)
+        match = match.astype(jnp.bfloat16)
+        wide = min(PICK, width)
+
+        def body(k, carry):
+            here = pl.ds(pl.multiple_of(k * wide, wide), wide)
+            routed[slot, :, here] = jnp.dot(
+                match, normed[:, here], preferred_element_type=jnp.float32
+            ).astype(jnp.bfloat16)
+            return carry
+
+        lax.fori_loop(0, width // wide, body, 0)
+
     def hid_block(u, zz):
         return hid.at[u, :, cols(zz * 2 + c)]
 
@@ -313,22 +325,10 @@
 
     def compute(u):
         p, j = u // local, u % local
-        s = source(p)
-        slot = jnp.minimum(p, 1)
-        match, _ = chosen(s, j)
-        match = match.astype(jnp.bfloat16)
-        wide = min(512, width)
-
-        def pick(k, carry):
-            here = pl.ds(pl.multiple_of(k * wide, wide), wide)
-            routed[:, here] = jnp.dot(
-                match, normed[slot, :, here], preferred_element_type=jnp.float32
-            ).astype(jnp.bfloat16)
-            return carry
-
-        lax.fori_loop(0, width // wide, pick, 0)
-        gate = jnp.dot(routed[...], wg[j], preferred_element_type=jnp.float32)
-        up = jnp.dot(routed[...], wu[j], preferred_element_type=jnp.float32)
+        lines_of = pl.ds(pl.multiple_of(j * CAP, CAP), CAP)
+        mine = routed[jnp.minimum(p, 1), lines_of, :]
+        gate = jnp.dot(mine, wg[j], preferred_element_type=jnp.float32)
+        up = jnp.dot(mine, wu[j], preferred_element_type=jnp.float32)
         hid[u, :, cols(t)] = clamped_unit(gate, up).astype(jnp.bfloat16)
 
         @pl.when(z < chips - 1)
@@ -420,7 +420,8 @@
             def _():
                 s = source(p)
                 from_partner(s)
-                normalise(s, jnp.minimum(p, 1))
+                normalise(s)
+                pick(s, jnp.minimum(p, 1))
 
             @pl.when(i < local)
             def _():
@@ -533,8 +534,8 @@
             pltpu.VMEM((local, width, columns), bf16),
             pltpu.VMEM((local, width, columns), bf16),
             pltpu.VMEM((2, width, columns), bf16),
-            pltpu.VMEM((2, rows, width), bf16),
-            pltpu.VMEM((CAP, width), bf16),
+            pltpu.VMEM((rows, width), bf16),
+            pltpu.VMEM((2, local * CAP, width), bf16),
             pltpu.VMEM((pieces, CAP, width), bf16),
             pltpu.VMEM((n_ep, local * CAP, columns), bf16),
             pltpu.VMEM((rows, columns), f32),
@@ -561,7 +562,7 @@
         ),
     )(
         tokens, norm_gain.reshape(1, columns), norm_bias.reshape(1, columns),
-        expert_ids, route_weights, gate_weight, up_weight, down_weight,
+        expert_ids.T, route_weights.T, gate_weight, up_weight, down_weight,
     )
 
 

time: 116 us -> 98.4 us (0.85)
  Pallas kernels: 111 us -> 96.6 us
  local copies, waits for them, and re-layouts: 4.5 us -> 1.62 us
    pallas_call x1, Pallas kernels: 111 us -> 96.6 us  [on_device(): pl.pallas_call(functools.partial(layer_kernel, side, n_tp, top), out_shap...]
    unnamed x3 -> x1, local copies, waits for them, and re-layouts: 4.5 us -> 1.62 us
where the time goes in v1:
time: 98.4 us; the launch traced here: 98.2 us
  Pallas kernels  96.6 us (98%)
  local copies, waits for them, and re-layouts  1.62 us (2%)
    pallas_call x1, Pallas kernels, on_device(): pl.pallas_call(functools.partial(layer_kernel, side, n_tp, top), out_shap...  96.6 us

profile of v1, /device:TPU:0, one launch (start us, length us, event | category | flops | bytes accessed | tf_op | source)
XLA Modules:
  0.0 98.2 jit_solution(3416327626833493521)
XLA Ops:
  0.0 96.6 %shard_map.82 = bf16[192,512]{1,0:T(8,128)(2,1)} custom-call(bf16[192,512]{1,0:T(8,128)(2,1)} %x_ref.1, f32[1,512]{1,0:T(1,128)} %bitcast.4, f32[1,512]{1,0:T(1,128)} %bitcast.5, s32[2,192]{1,0:T(2,128)} %bitcast.6, f32[2,192]{1,0:T(2,128)} %bitcast.7, bf16[4,4096,512]{2,1,0:T(8,128)(2,1)} %gate_hbm.1, bf16[4,4096,512]{2,1,0:T(8,128)(2,1)} %up_hbm.1, ...), custom_call_target="tpu_custom_call" | custom-call | tf_op jit(solution)/shard_map/pallas_call | solution.py:522
  96.6 1.6 %copy.10 = bf16[192,512]{1,0:T(8,128)(2,1)} copy(bf16[192,512]{1,0:T(8,128)(2,1)} %shard_map.82) | data formatting | bytes 393216
